TPU v7x, 256 devices: a whole 4x4x8 slice. The times are simulated.
256 devices in a mesh: ep: 64 (over z, y, core), tp: 4 (over x).
Axes of the slice: x: 4, y: 4, z: 8, core: 2. Of those that a mesh axis runs over, the one named last changes fastest.
Arguments:
- c_gate: bfloat16 [16384, 1024], P('ep', 'tp'), may hold values from -6 to 6
- b_gate: bfloat16 [16384, 1024], P('ep', 'tp'), may hold values from -6 to 6
- values: bfloat16 [16384, 1024], P('ep', 'tp'), may hold values from -6 to 6
- conv_taps: float32 [3, 1024], P(None, 'tp'), may hold values from -3.5 to 3.5
- w_mix_out: bfloat16 [1024, 2048], P('tp'), may hold values from -0.1875 to 0.1875
- moe_in: bfloat16 [32768, 2048], P(('ep', 'tp')), may hold values from -6 to 6
- norm_gain: float32 [2048], replicated, may hold values from 0.1 to 1.9
- route_ids: int32 [32768, 2], P(('ep', 'tp')), may hold values from 0 to 63, all different within a row; in each aligned block of 128 rows (0 to 127, 128 to 255, ...) at most 5 rows name the same one
- route_weights: float32 [32768, 2], P(('ep', 'tp')), may hold values from 0.1 to 1
- w_gate: bfloat16 [64, 2048, 3584], P('ep', None, 'tp'), may hold values from -0.125 to 0.125
- w_up: bfloat16 [64, 2048, 3584], P('ep', None, 'tp'), may hold values from -0.125 to 0.125
- w_down: bfloat16 [64, 3584, 2048], P('ep', 'tp'), may hold values from -0.09375 to 0.09375
Outputs:
- mixer_out: bfloat16 [16384, 2048], P(('ep', 'tp'))
- moe_out: bfloat16 [32768, 2048], P(('ep', 'tp'))
Inputs may be any that keep to these rules, and one draw needn't show every extreme that they name: `route_ids`: each row names 2 different experts; in each aligned block of 128 rows (the rows of one device) no expert is named by more than 5 rows, and in every draw some expert is named by exactly 5 rows in some block.
All inputs are finite; a program needn't handle non-finite values.
Results may differ from a plain program's by a relative error of at most 0.012.
Values may be sent and summed in bfloat16 or wider, within the bound.
No kernel may reach another device: no remote copies, remote signals or barrier semaphores. Data moves between devices by JAX's collectives and lax.ppermute only.
A program may use at most 128 MiB of HBM per device.

v0:
```python
import jax
import jax.numpy as jnp
from jax import lax
from jax.sharding import PartitionSpec as P

EPS = 1e-06


def passed_along(block, axis, distance):
    devices = range(lax.axis_size(axis))
    route = [(i - distance, i) for i in devices if i - distance in devices]
    return lax.ppermute(block, axis, route)


def split_up(shard, dim, length):
    before, after = (shard.shape[:dim], shard.shape[dim + 1 :])
    return jnp.moveaxis(shard.reshape(*before, length, -1, *after), dim, 0)


def sent_and_summed(shard, axis, dim):
    blocks = split_up(shard, dim, lax.axis_size(axis))
    arrived = lax.all_to_all(blocks, axis, split_axis=0, concat_axis=0, tiled=True)
    return arrived.astype(jnp.float32).sum(axis=0)


def rank_copies(route_block, experts):
    flat_ids = route_block.reshape(-1)
    onehot = (flat_ids[:, None] == jnp.arange(experts, dtype=jnp.int32)[None, :]).astype(jnp.int32)
    before = jnp.cumsum(onehot, axis=0) - onehot
    return (flat_ids, jnp.sum(before * onehot, axis=1))


def pack_rows(rows, slot_of, top, slot_count):
    copies = slot_of.shape[0]
    table = (
        jnp.full((slot_count,), copies, jnp.int32)
        .at[slot_of]
        .set(jnp.arange(copies, dtype=jnp.int32))
    )
    padded = jnp.concatenate([rows, jnp.zeros((1, rows.shape[1]), rows.dtype)], 0)
    return padded[table // top]


def on_device(
    c_gate,
    b_gate,
    values,
    conv_taps,
    w_mix_out,
    moe_in,
    norm_gain,
    route_ids,
    route_weights,
    w_gate,
    w_up,
    w_down,
):
    tokens = c_gate.shape[0]
    reach = conv_taps.shape[0] - 1
    product = c_gate.astype(jnp.float32) * values.astype(jnp.float32)
    previous = passed_along(product[tokens - reach :], "ep", 1)
    extended = jnp.concatenate([previous, product], 0)
    convolved = jnp.zeros_like(product)
    for offset in range(reach + 1):
        convolved = convolved + conv_taps[offset][None, :] * extended[offset : offset + tokens]
    mixed = (b_gate.astype(jnp.float32) * convolved).astype(jnp.bfloat16)
    piece = mixed
    mixer_out = sent_and_summed(
        jnp.dot(piece, w_mix_out, preferred_element_type=jnp.float32).astype(jnp.bfloat16), "tp", 0
    ).astype(jnp.bfloat16)
    rows_b = moe_in.shape[0]
    width = moe_in.shape[1]
    top = route_ids.shape[1]
    n_ep = lax.axis_size("ep")
    experts = w_gate.shape[0] * n_ep
    capacity = 5 * rows_b * top // (4 * experts)
    stream = moe_in.astype(jnp.float32)
    scale = lax.rsqrt(jnp.mean(stream * stream, axis=1, keepdims=True) + EPS)
    normed = (stream * scale * norm_gain[None, :]).astype(jnp.bfloat16)
    own_ids, own_ranks = rank_copies(route_ids, experts)
    own_slot = own_ids * capacity + own_ranks
    outgoing = pack_rows(normed, own_slot, top, experts * capacity).reshape(
        experts, capacity, width
    )
    arrived = lax.all_to_all(outgoing, "ep", split_axis=0, concat_axis=1, tiled=True).reshape(
        -1, width
    )
    piece = lax.all_gather(arrived, "tp", axis=0, tiled=True)
    gate_val = jnp.dot(piece, w_gate[0], preferred_element_type=jnp.float32)
    up_val = jnp.dot(piece, w_up[0], preferred_element_type=jnp.float32)
    hidden = (jax.nn.silu(gate_val) * up_val).astype(jnp.bfloat16)
    piece = hidden
    expert_out = sent_and_summed(
        jnp.dot(piece, w_down[0], preferred_element_type=jnp.float32).astype(jnp.bfloat16), "tp", 0
    ).astype(jnp.bfloat16)
    returned = lax.all_to_all(
        expert_out.reshape(n_ep, capacity, width), "ep", split_axis=0, concat_axis=0, tiled=True
    )
    picked = returned.reshape(-1, width)[own_slot].astype(jnp.float32).reshape(rows_b, top, width)
    moe_out = jnp.sum(picked * route_weights[:, :, None], axis=1).astype(jnp.bfloat16)
    return (mixer_out, moe_out)


def solution(mesh):
    return jax.shard_map(
        on_device,
        mesh=mesh,
        in_specs=(
            P("ep", "tp"),
            P("ep", "tp"),
            P("ep", "tp"),
            P(None, "tp"),
            P("tp", None),
            P(("ep", "tp"), None),
            P(),
            P(("ep", "tp"), None),
            P(("ep", "tp"), None),
            P("ep", None, "tp"),
            P("ep", None, "tp"),
            P("ep", "tp", None),
        ),
        out_specs=(P(("ep", "tp"), None), P(("ep", "tp"), None)),
        check_vma=False,
    )
```

profile of v0, /device:TPU:8, one launch (start us, length us, event | category | flops | bytes accessed | tf_op | source)
XLA Modules:
  0.0 333.2 jit_solution(17508996634302096302)
XLA Ops:
  7.2 0.0 copy-start
  7.2 0.0 all-gather.2.cloned.1.call-start
  7.2 0.9 copy.16
  8.1 0.1 eq.29
  8.2 0.1 eq.25
  8.4 0.7 broadcast_multiply_fusion
  9.1 0.6 reduce-window.6
  9.7 0.2 slice_reduce_fusion
  9.9 0.1 copy.15
  10.0 0.1 mul.107
  10.2 0.1 fusion.20
  10.3 1.4 scatter_custom_fusion
  11.7 1.2 fusion.4
  13.0 1.2 fusion.6
  14.3 3.0 gather_fusion
  17.3 2.4 reshape.88
  19.7 63.2 %all_to_all.24 = bf16[64,5,2048]{2,1,0:T(8,128)(2,1)} all-to-all(bf16[64,5,2048]{2,1,0:T(8,128)(2,1)S(1)} %reshape.88), channel_id=1, replica_groups=mesh['ep'=64,'tp'=4] {'ep'}, dimensions={0} | all-to-all | bytes 2621440 | tf_op jit(solution)/shard_map/all_to_all | solution.py:85
  82.9 3.7 %reshape.89 = bf16[320,2048]{1,0:T(8,128)(2,1)} reshape(bf16[64,5,2048]{2,1,0:T(8,128)(2,1)} %all_to_all.24) | data formatting | bytes 2621440 | tf_op jit(solution)/shard_map/reshape | solution.py:85
  86.6 0.0 all-gather.2.cloned.1.call-update
  86.6 55.8 %all-gather.2.cloned.1.call-done = bf16[1280,2048]{1,0:T(8,128)(2,1)} async-done(((bf16[320,2048]{1,0:T(8,128)(2,1)}), bf16[1280,2048]{1,0:T(8,128)(2,1)}) %all-gather.2.cloned.1.call-update) | async-done | bytes 5242896 | tf_op jit(solution)/shard_map/all_gather | solution.py:88
  142.4 10.0 %fusion.2 = f32[1280,896]{1,0:T(8,128)} fusion(bf16[1280,2048]{1,0:T(8,128)(2,1)} %all-gather.2.cloned.1.call-done, bf16[1,2048,896]{2,1,0:T(8,128)(2,1)} %param.21), kind=kOutput, calls=%fused_computation.7 | convolution fusion | flops 4697620480 | bytes 13500416 | tf_op jit(solution)/shard_map/dot_general | solution.py:89
  152.4 17.5 %convolution_convert_fusion = bf16[1280,2048]{1,0:T(8,128)(2,1)} fusion(bf16[1,896,2048]{2,1,0:T(8,128)(2,1)} %param.23, f32[1280,896]{1,0:T(8,128)} %fusion.2, bf16[1280,2048]{1,0:T(8,128)(2,1)} %all-gather.2.cloned.1.call-done, bf16[1,2048,896]{2,1,0:T(8,128)(2,1)} %param.22), kind=kOutput, calls=%fused_computation.3 | convolution fusion | flops 9404743680 | bytes 22413312 | tf_op jit(solution)/shard_map/dot_general | solution.py:94
  169.9 0.0 copy-start.2
  169.9 0.0 copy-start.1
  169.9 5.2 %all-to-all-start.2 = ((bf16[4,320,2048]{2,1,0:T(8,128)(2,1)}), bf16[4,320,2048]{2,1,0:T(8,128)(2,1)}, u32[]{:S(2)}, u32[]{:S(2)}) async-start(bf16[4,320,2048]{2,1,0:T(8,128)(2,1)} %bitcast.47), calls=%async_computation.2 | async-start | bytes 10485760 | tf_op jit(solution)/shard_map/all_to_all | solution.py:22
  175.1 0.0 copy-done.2
  175.2 0.0 copy-done.3
  175.2 1.9 collective-permute-start
  177.1 0.0 copy-done.4
  177.2 3.0 collective-permute-done
  180.1 0.0 copy-done
  180.1 0.0 copy-done.1
  180.1 1.5 convolution_convert_fusion.1
  181.6 53.8 %all-to-all-done.2 = bf16[4,320,2048]{2,1,0:T(8,128)(2,1)} async-done(((bf16[4,320,2048]{2,1,0:T(8,128)(2,1)}), bf16[4,320,2048]{2,1,0:T(8,128)(2,1)}, u32[]{:S(2)}, u32[]{:S(2)}) %all-to-all-start.2) | async-done | bytes 5242912 | tf_op jit(solution)/shard_map/all_to_all | solution.py:22
  235.4 3.7 %all-to-all-start = ((bf16[4,64,2048]{2,1,0:T(8,128)(2,1)}), bf16[4,64,2048]{2,1,0:T(8,128)(2,1)S(1)}, u32[]{:S(2)}, u32[]{:S(2)}) async-start(bf16[4,64,2048]{2,1,0:T(8,128)(2,1)} %bitcast.3), calls=%async_computation | async-start | bytes 2097152 | tf_op jit(solution)/shard_map/all_to_all | solution.py:22
  239.1 3.6 %reduce_sum.57 = bf16[320,2048]{1,0:T(8,128)(2,1)S(1)} reduce(bf16[4,320,2048]{2,1,0:T(8,128)(2,1)} %all-to-all-done.2, bf16[]{:T(256)} %constant.18.clone.1), dimensions={0}, to_apply=%region_6.7 | reduce | flops 1966080 | bytes 6553602 | tf_op jit(solution)/shard_map/reduce_sum | solution.py:23
  242.7 0.0 copy-start.5
  242.7 1.6 reshape.91
  244.3 8.9 %all-to-all-done = bf16[4,64,2048]{2,1,0:T(8,128)(2,1)S(1)} async-done(((bf16[4,64,2048]{2,1,0:T(8,128)(2,1)}), bf16[4,64,2048]{2,1,0:T(8,128)(2,1)S(1)}, u32[]{:S(2)}, u32[]{:S(2)}) %all-to-all-start) | async-done | bytes 1048608 | tf_op jit(solution)/shard_map/all_to_all | solution.py:22
  253.2 10.7 %all-to-all-start.3 = ((bf16[64,5,2048]{2,1,0:T(8,128)(2,1)}), bf16[64,5,2048]{2,1,0:T(8,128)(2,1)}, u32[]{:S(2)}, u32[]{:S(2)}) async-start(bf16[64,5,2048]{2,1,0:T(8,128)(2,1)} %reshape.91), calls=%async_computation.3 | async-start | bytes 4194304 | tf_op jit(solution)/shard_map/all_to_all | solution.py:96
  263.9 0.0 copy-done.5
  264.0 0.1 copy.19
  264.1 0.9 reduce_sum.53
  265.0 50.1 %all-to-all-done.3 = bf16[64,5,2048]{2,1,0:T(8,128)(2,1)} async-done(((bf16[64,5,2048]{2,1,0:T(8,128)(2,1)}), bf16[64,5,2048]{2,1,0:T(8,128)(2,1)}, u32[]{:S(2)}, u32[]{:S(2)}) %all-to-all-start.3) | async-done | bytes 1310752 | tf_op jit(solution)/shard_map/all_to_all | solution.py:96
  315.1 2.6 reshape.92
  317.7 2.3 gather_fusion.1
  320.0 2.4 reshape.93
  322.4 3.9 %multiply_reduce_fusion = bf16[128,2048]{1,0:T(8,128)(2,1)} fusion(f32[128,2,2048]{2,1,0:T(2,128)S(1)} %reshape.93, f32[128,2]{1,0:T(8,128)S(1)} %copy.19), kind=kLoop, calls=%fused_computation.10 | loop fusion | flops 786432 | bytes 2622464 | tf_op jit(solution)/shard_map/reduce_sum | solution.py:100
  (15 shorter events, 0.2 us)
Async XLA Ops:
  7.2 173.0 %copy-start = (bf16[256,2048]{1,0:T(8,128)(2,1)S(1)}, bf16[256,2048]{1,0:T(8,128)(2,1)}, u32[]{:S(2)}) copy-start(bf16[256,2048]{1,0:T(8,128)(2,1)} %param.16) | copy-start | bytes 3145732
  7.2 135.2 %all-gather.2.cloned.1.call-start = ((), (), s32[]{:S(2)}) async-start(), calls=%async_computation.4 | async-start | bytes 6553600 | tf_op jit(solution)/shard_map/all_gather | solution.py:88
  169.9 5.3 %copy-start.2 = (bf16[256,256]{1,0:T(8,128)(2,1)S(1)}, bf16[256,256]{1,0:T(8,128)(2,1)}, u32[]{:S(2)}) copy-start(bf16[256,256]{1,0:T(8,128)(2,1)} %param.14) | copy-start | bytes 393220
  169.9 5.3 %copy-start.3 = (bf16[256,256]{1,0:T(8,128)(2,1)S(1)}, bf16[256,256]{1,0:T(8,128)(2,1)}, u32[]{:S(2)}) copy-start(bf16[256,256]{1,0:T(8,128)(2,1)} %param.12) | copy-start | bytes 393220
  169.9 7.2 %copy-start.4 = (f32[3,256]{1,0:T(4,128)S(1)}, f32[3,256]{1,0:T(4,128)}, u32[]{:S(2)}) copy-start(f32[3,256]{1,0:T(4,128)} %param.15) | copy-start | bytes 9220
  169.9 10.2 %copy-start.1 = (bf16[256,256]{1,0:T(8,128)(2,1)S(1)}, bf16[256,256]{1,0:T(8,128)(2,1)}, u32[]{:S(2)}) copy-start(bf16[256,256]{1,0:T(8,128)(2,1)} %param.13) | copy-start | bytes 393220
  169.9 65.4 %all-to-all-start.2 = ((bf16[4,320,2048]{2,1,0:T(8,128)(2,1)}), bf16[4,320,2048]{2,1,0:T(8,128)(2,1)}, u32[]{:S(2)}, u32[]{:S(2)}) async-start(bf16[4,320,2048]{2,1,0:T(8,128)(2,1)} %bitcast.47), calls=%async_computation.2 | async-start | bytes 10485760 | tf_op jit(solution)/shard_map/all_to_all | solution.py:22
  175.2 4.9 %collective-permute-start = (f32[2,256]{1,0:T(2,128)S(1)}, f32[2,256]{1,0:T(2,128)S(1)}, u32[]{:S(2)}, u32[]{:S(2)}) collective-permute-start(f32[2,256]{1,0:T(2,128)S(1)} %slice.36), channel_id=1, source_target_pairs={{0,4},{4,8},{8,12},{12,16},{16,20},{20,24},{24,28},{28,32},{32,36}... | collective-permute-start | bytes 6152 | tf_op jit(solution)/shard_map/ppermute | solution.py:12
  235.4 17.8 %all-to-all-start = ((bf16[4,64,2048]{2,1,0:T(8,128)(2,1)}), bf16[4,64,2048]{2,1,0:T(8,128)(2,1)S(1)}, u32[]{:S(2)}, u32[]{:S(2)}) async-start(bf16[4,64,2048]{2,1,0:T(8,128)(2,1)} %bitcast.3), calls=%async_computation | async-start | bytes 2097152 | tf_op jit(solution)/shard_map/all_to_all | solution.py:22
  242.7 21.3 %copy-start.5 = (f32[128,2]{0,1:T(2,128)S(1)}, f32[128,2]{0,1:T(2,128)}, u32[]{:S(2)}) copy-start(f32[128,2]{0,1:T(2,128)} %param.20) | copy-start | bytes 3076
  253.2 61.9 %all-to-all-start.3 = ((bf16[64,5,2048]{2,1,0:T(8,128)(2,1)}), bf16[64,5,2048]{2,1,0:T(8,128)(2,1)}, u32[]{:S(2)}, u32[]{:S(2)}) async-start(bf16[64,5,2048]{2,1,0:T(8,128)(2,1)} %reshape.91), calls=%async_computation.3 | async-start | bytes 4194304 | tf_op jit(solution)/shard_map/all_to_all | solution.py:96
Sparse Core Ops, SparseCore 0:
  86.7 55.6 all-gather.1
where the time goes:
time: 334 us; the launch traced here: 333 us
  waiting for transfers between devices  172 us (51%)
  blocking collectives  63.2 us (19%)
  matrix products  29 us (9%)
  starting transfers between devices  21.6 us (6%)
  local copies, waits for them, and re-layouts  21.1 us (6%)
  between operations  14.2 us (4%)
  other arithmetic  12.4 us (4%)
    all_to_all x1, blocking collectives, on_device(): lax.all_to_all(outgoing, 'ep', split_axis=0, concat_axis=1, tiled=True)  63.2 us
    all_to_all x2, waiting for transfers between devices, sent_and_summed(): lax.all_to_all(blocks, axis, split_axis=0, concat_axis=0, tiled=True)  62.6 us
    all_gather x1, waiting for transfers between devices, on_device(): piece = lax.all_gather(arrived, 'tp', axis=0, tiled=True)  55.8 us
    all_to_all x1, waiting for transfers between devices, on_device(): lax.all_to_all(expert_out.reshape(n_ep, capacity, width), 'ep', split_axi...  50.1 us
    dot_general x1, matrix products, on_device(): jnp.dot(piece, w_down[0], preferred_element_type=jnp.float32)  17.5 us
    all_to_all x1, starting transfers between devices, on_device(): lax.all_to_all(expert_out.reshape(n_ep, capacity, width), 'ep', split_axi...  10.7 us
    dot_general x1, matrix products, on_device(): gate_val = jnp.dot(piece, w_gate[0], preferred_element_type=jnp.float32)  9.98 us
    all_to_all x2, starting transfers between devices, sent_and_summed(): lax.all_to_all(blocks, axis, split_axis=0, concat_axis=0, tiled=True)  8.91 us
  transfers between devices with their start and end apart: 5, of which 5 were waited for; matrix products, arithmetic and copies ran while one was open for 2% of the time, Pallas kernels for 0%

commit v1 on v0

--- a/solution.py
+++ b/solution.py
@@ -4,6 +4,24 @@
 from jax.sharding import PartitionSpec as P
 
 EPS = 1e-06
+
+
+def collect(shard, axis, dim):
+    ways, here, step = (lax.axis_size(axis), lax.axis_index(axis), shard.shape[dim])
+    lengths = [n * ways if d == dim else n for d, n in enumerate(shard.shape)]
+    full = lax.dynamic_update_slice_in_dim(
+        jnp.zeros(lengths, shard.dtype), shard, here * step, axis=dim
+    )
+    going_up = going_down = shard
+    for far in range(1, ways // 2 + 1):
+        going_up = lax.ppermute(going_up, axis, [(d, (d + 1) % ways) for d in range(ways)])
+        full = lax.dynamic_update_slice_in_dim(full, going_up, (here - far) % ways * step, axis=dim)
+        if 2 * far < ways:
+            going_down = lax.ppermute(going_down, axis, [(d, (d - 1) % ways) for d in range(ways)])
+            full = lax.dynamic_update_slice_in_dim(
+                full, going_down, (here + far) % ways * step, axis=dim
+            )
+    return full
 
 
 def passed_along(block, axis, distance):
@@ -85,7 +103,7 @@
     arrived = lax.all_to_all(outgoing, "ep", split_axis=0, concat_axis=1, tiled=True).reshape(
         -1, width
     )
-    piece = lax.all_gather(arrived, "tp", axis=0, tiled=True)
+    piece = collect(arrived, "tp", 0)
     gate_val = jnp.dot(piece, w_gate[0], preferred_element_type=jnp.float32)
     up_val = jnp.dot(piece, w_up[0], preferred_element_type=jnp.float32)
     hidden = (jax.nn.silu(gate_val) * up_val).astype(jnp.bfloat16)

time: 334 us -> 322 us (0.964)
  between operations: 14.2 us -> 0.93 us
  waiting for transfers between devices: 172 us -> 162 us
  starting transfers between devices: 21.6 us -> 28.9 us
  local copies, waits for them, and re-layouts: 21.1 us -> 27.7 us
    all_gather x1 -> x0, waiting for transfers between devices: 55.8 us -> none  [on_device(): piece = lax.all_gather(arrived, 'tp', axis=0, tiled=True)]
    ppermute x0 -> x3, waiting for transfers between devices: none -> 52.5 us  [the longest x2 52.5 us: collect(): lax.ppermute(going_up, axis, [(d, (d + 1) % ways) for d in range(ways)])]
    all_to_all x2, waiting for transfers between devices: 62.6 us -> 56.7 us  [sent_and_summed(): lax.all_to_all(blocks, axis, split_axis=0, concat_axis=0, tiled=True)]
    dynamic_update_slice x0 -> x4, local copies, waits for them, and re-layouts: none -> 4.71 us  [the longest x2 3.08 us: collect(): lax.dynamic_update_slice_in_dim(full, going_up, (here - far) % ways * ste...]
    all_to_all x1, starting transfers between devices: 10.7 us -> 14.6 us  [on_device(): lax.all_to_all(expert_out.reshape(n_ep, capacity, width), 'ep', split_axi...]
    ppermute x0 -> x3, starting transfers between devices: none -> 3.59 us  [the longest x2 1.85 us: collect(): lax.ppermute(going_up, axis, [(d, (d + 1) % ways) for d in range(ways)])]
  transfers between devices with their start and end apart: 5 -> 7, of which waited for: 5 -> 6; matrix products, arithmetic and copies ran while one was open for 2% -> 4% of each run, Pallas kernels for 0% -> 0%
where the time goes in v1:
time: 322 us
  waiting for transfers between devices  162 us (50%)
  blocking collectives  63.2 us (20%)
  starting transfers between devices  28.9 us (9%)
  local copies, waits for them, and re-layouts  27.7 us (9%)
  matrix products  26.1 us (8%)
  other arithmetic  12.4 us (4%)
    all_to_all x1, blocking collectives, on_device(): lax.all_to_all(outgoing, 'ep', split_axis=0, concat_axis=1, tiled=True)  63.2 us
    all_to_all x2, waiting for transfers between devices, sent_and_summed(): lax.all_to_all(blocks, axis, split_axis=0, concat_axis=0, tiled=True)  56.7 us
    ppermute x2, waiting for transfers between devices, collect(): lax.ppermute(going_up, axis, [(d, (d + 1) % ways) for d in range(ways)])  52.5 us
    all_to_all x1, waiting for transfers between devices, on_device(): lax.all_to_all(expert_out.reshape(n_ep, capacity, width), 'ep', split_axi...  50.1 us
    dot_general x1, matrix products, on_device(): jnp.dot(piece, w_down[0], preferred_element_type=jnp.float32)  17.5 us
    all_to_all x1, starting transfers between devices, on_device(): lax.all_to_all(expert_out.reshape(n_ep, capacity, width), 'ep', split_axi...  14.6 us
    all_to_all x2, starting transfers between devices, sent_and_summed(): lax.all_to_all(blocks, axis, split_axis=0, concat_axis=0, tiled=True)  8.73 us
    dot_general x1, matrix products, on_device(): gate_val = jnp.dot(piece, w_gate[0], preferred_element_type=jnp.float32)  7.17 us
  transfers between devices with their start and end apart: 7, of which 6 were waited for; matrix products, arithmetic and copies ran while one was open for 4% of the time, Pallas kernels for 0%

profile of v1, /device:TPU:8, one launch (start us, length us, event | category | flops | bytes accessed | tf_op | source)
XLA Modules:
  0.0 321.6 jit_solution(17783379644367424700)
XLA Ops:
  0.6 0.0 copy-start
  0.6 0.9 copy.16
  1.5 0.1 eq.33
  1.7 0.1 eq.29
  1.8 0.7 broadcast_multiply_fusion
  2.5 0.6 reduce-window.6
  3.1 0.2 slice_reduce_fusion
  3.3 0.1 copy.15
  3.5 0.1 mul.119
  3.6 0.1 fusion.23
  3.7 1.4 scatter_custom_fusion
  5.2 1.2 fusion.7
  6.4 1.2 fusion.9
  7.7 3.0 gather_fusion
  10.7 2.4 reshape.88
  13.1 63.2 %all_to_all.24 = bf16[64,5,2048]{2,1,0:T(8,128)(2,1)} all-to-all(bf16[64,5,2048]{2,1,0:T(8,128)(2,1)S(1)} %reshape.88), channel_id=1, replica_groups=mesh['ep'=64,'tp'=4] {'ep'}, dimensions={0} | all-to-all | bytes 2621440 | tf_op jit(solution)/shard_map/all_to_all | solution.py:103
  76.3 2.6 reshape.89
  78.9 1.6 collective-permute-start.1
  80.5 1.7 collective-permute-start.2
  82.2 27.1 %collective-permute-done.1 = bf16[320,2048]{1,0:T(8,128)(2,1)} collective-permute-done((bf16[320,2048]{1,0:T(8,128)(2,1)S(1)}, bf16[320,2048]{1,0:T(8,128)(2,1)}, u32[]{:S(2)}, u32[]{:S(2)}) %collective-permute-start.1) | collective-permute-done | bytes 1310752 | tf_op jit(solution)/shard_map/ppermute | solution.py:17
  109.3 0.3 collective-permute-start.3
  109.6 0.6 broadcast_in_dim.6
  110.2 0.2 constant_dynamic-update-slice_fusion.3
  110.4 1.6 constant_dynamic-update-slice_fusion.2
  112.0 1.5 constant_dynamic-update-slice_fusion.1
  113.5 25.4 %collective-permute-done.3 = bf16[320,2048]{1,0:T(8,128)(2,1)} collective-permute-done((bf16[320,2048]{1,0:T(8,128)(2,1)}, bf16[320,2048]{1,0:T(8,128)(2,1)}, u32[]{:S(2)}, u32[]{:S(2)}) %collective-permute-start.3) | collective-permute-done | bytes 1310752 | tf_op jit(solution)/shard_map/ppermute | solution.py:17
  139.0 1.5 constant_dynamic-update-slice_fusion
  140.4 2.3 copy-done.1
  142.8 7.2 %fusion.5 = f32[1280,896]{1,0:T(8,128)} fusion(bf16[1280,2048]{1,0:T(8,128)(2,1)S(1)} %constant_dynamic-update-slice_fusion, bf16[1,2048,896]{2,1,0:T(8,128)(2,1)S(1)} %copy-done.7), kind=kOutput, calls=%fused_computation.8 | convolution fusion | flops 4697620480 | bytes 13500416 | tf_op jit(solution)/shard_map/dot_general | solution.py:107
  150.0 17.5 %convolution_convert_fusion = bf16[1280,2048]{1,0:T(8,128)(2,1)} fusion(bf16[1,896,2048]{2,1,0:T(8,128)(2,1)} %param.23, f32[1280,896]{1,0:T(8,128)} %fusion.5, bf16[1280,2048]{1,0:T(8,128)(2,1)} %copy-done.1, bf16[1,2048,896]{2,1,0:T(8,128)(2,1)} %param.22), kind=kOutput, calls=%fused_computation.3 | convolution fusion | flops 9404743680 | bytes 22413312 | tf_op jit(solution)/shard_map/dot_general | solution.py:112
  167.5 5.2 %all-to-all-start.2 = ((bf16[4,320,2048]{2,1,0:T(8,128)(2,1)}), bf16[4,320,2048]{2,1,0:T(8,128)(2,1)}, u32[]{:S(2)}, u32[]{:S(2)}) async-start(bf16[4,320,2048]{2,1,0:T(8,128)(2,1)} %bitcast.49), calls=%async_computation.2 | async-start | bytes 10485760 | tf_op jit(solution)/shard_map/all_to_all | solution.py:40
  172.8 1.9 collective-permute-start
  174.8 3.0 collective-permute-done
  177.7 1.5 convolution_convert_fusion.1
  179.2 50.7 %all-to-all-done.2 = bf16[4,320,2048]{2,1,0:T(8,128)(2,1)} async-done(((bf16[4,320,2048]{2,1,0:T(8,128)(2,1)}), bf16[4,320,2048]{2,1,0:T(8,128)(2,1)}, u32[]{:S(2)}, u32[]{:S(2)}) %all-to-all-start.2) | async-done | bytes 5242912 | tf_op jit(solution)/shard_map/all_to_all | solution.py:40
  229.9 3.5 %all-to-all-start = ((bf16[4,64,2048]{2,1,0:T(8,128)(2,1)}), bf16[4,64,2048]{2,1,0:T(8,128)(2,1)S(1)}, u32[]{:S(2)}, u32[]{:S(2)}) async-start(bf16[4,64,2048]{2,1,0:T(8,128)(2,1)} %bitcast.3), calls=%async_computation | async-start | bytes 2097152 | tf_op jit(solution)/shard_map/all_to_all | solution.py:40
  233.4 3.6 %reduce_sum.57 = bf16[320,2048]{1,0:T(8,128)(2,1)S(1)} reduce(bf16[4,320,2048]{2,1,0:T(8,128)(2,1)} %all-to-all-done.2, bf16[]{:T(256)} %constant.58.clone.1), dimensions={0}, to_apply=%region_6.7 | reduce | flops 1966080 | bytes 6553602 | tf_op jit(solution)/shard_map/reduce_sum | solution.py:41
  237.0 0.0 copy-start.6
  237.0 1.6 reshape.91
  238.7 6.0 %all-to-all-done = bf16[4,64,2048]{2,1,0:T(8,128)(2,1)S(1)} async-done(((bf16[4,64,2048]{2,1,0:T(8,128)(2,1)}), bf16[4,64,2048]{2,1,0:T(8,128)(2,1)S(1)}, u32[]{:S(2)}, u32[]{:S(2)}) %all-to-all-start) | async-done | bytes 1048608 | tf_op jit(solution)/shard_map/all_to_all | solution.py:40
  244.7 14.6 %all-to-all-start.3 = ((bf16[64,5,2048]{2,1,0:T(8,128)(2,1)}), bf16[64,5,2048]{2,1,0:T(8,128)(2,1)}, u32[]{:S(2)}, u32[]{:S(2)}) async-start(bf16[64,5,2048]{2,1,0:T(8,128)(2,1)} %reshape.91), calls=%async_computation.3 | async-start | bytes 4194304 | tf_op jit(solution)/shard_map/all_to_all | solution.py:114
  259.3 0.1 copy.19
  259.4 0.9 reduce_sum.53
  260.3 50.1 %all-to-all-done.3 = bf16[64,5,2048]{2,1,0:T(8,128)(2,1)} async-done(((bf16[64,5,2048]{2,1,0:T(8,128)(2,1)}), bf16[64,5,2048]{2,1,0:T(8,128)(2,1)}, u32[]{:S(2)}, u32[]{:S(2)}) %all-to-all-start.3) | async-done | bytes 1310752 | tf_op jit(solution)/shard_map/all_to_all | solution.py:114
  310.4 2.6 reshape.92
  313.0 2.3 gather_fusion.1
  315.3 2.4 reshape.93
  317.7 3.9 %multiply_reduce_fusion = bf16[128,2048]{1,0:T(8,128)(2,1)} fusion(f32[128,2,2048]{2,1,0:T(2,128)S(1)} %reshape.93, f32[128,2]{1,0:T(8,128)S(1)} %copy.19), kind=kLoop, calls=%fused_computation.11 | loop fusion | flops 786432 | bytes 2622464 | tf_op jit(solution)/shard_map/reduce_sum | solution.py:118
  (27 shorter events, 0.2 us)
Async XLA Ops:
  0.6 177.1 %copy-start = (bf16[256,2048]{1,0:T(8,128)(2,1)S(1)}, bf16[256,2048]{1,0:T(8,128)(2,1)}, u32[]{:S(2)}) copy-start(bf16[256,2048]{1,0:T(8,128)(2,1)} %param.16) | copy-start | bytes 3145732
  78.9 30.4 %collective-permute-start.1 = (bf16[320,2048]{1,0:T(8,128)(2,1)S(1)}, bf16[320,2048]{1,0:T(8,128)(2,1)}, u32[]{:S(2)}, u32[]{:S(2)}) collective-permute-start(bf16[320,2048]{1,0:T(8,128)(2,1)S(1)} %reshape.89), channel_id=1, source_target_pairs={{0,1},{1,2},{2,3},{3,0},{4,5},{5,6},{6,7},{7,4},{8,9},{9,10},{10,1... | collective-permute-start | bytes 3932168 | tf_op jit(solution)/shard_map/ppermute | solution.py:17
  80.5 31.6 %collective-permute-start.2 = (bf16[320,2048]{1,0:T(8,128)(2,1)S(1)}, bf16[320,2048]{1,0:T(8,128)(2,1)}, u32[]{:S(2)}, u32[]{:S(2)}) collective-permute-start(bf16[320,2048]{1,0:T(8,128)(2,1)S(1)} %reshape.89), channel_id=1, source_target_pairs={{0,3},{1,0},{2,1},{3,2},{4,7},{5,4},{6,5},{7,6},{8,11},{9,8},{10,9... | collective-permute-start | bytes 3932168 | tf_op jit(solution)/shard_map/ppermute | solution.py:20
  109.3 29.7 %collective-permute-start.3 = (bf16[320,2048]{1,0:T(8,128)(2,1)}, bf16[320,2048]{1,0:T(8,128)(2,1)}, u32[]{:S(2)}, u32[]{:S(2)}) collective-permute-start(bf16[320,2048]{1,0:T(8,128)(2,1)} %collective-permute-done.1), channel_id=1, source_target_pairs={{0,1},{1,2},{2,3},{3,0},{4,5},{5,6},{6,7},{7,4},{8,9},{9,10},{10,1... | collective-permute-start | bytes 3932168 | tf_op jit(solution)/shard_map/ppermute | solution.py:17
  110.4 32.4 %copy-start.7 = (bf16[1,2048,896]{2,1,0:T(8,128)(2,1)S(1)}, bf16[1,2048,896]{2,1,0:T(8,128)(2,1)}, u32[]{:S(2)}) copy-start(bf16[1,2048,896]{2,1,0:T(8,128)(2,1)} %param.21) | copy-start | bytes 11010052
  140.4 2.4 copy-start.1
  167.5 5.3 %copy-start.3 = (bf16[256,256]{1,0:T(8,128)(2,1)S(1)}, bf16[256,256]{1,0:T(8,128)(2,1)}, u32[]{:S(2)}) copy-start(bf16[256,256]{1,0:T(8,128)(2,1)} %param.14) | copy-start | bytes 393220
  167.5 5.3 %copy-start.4 = (bf16[256,256]{1,0:T(8,128)(2,1)S(1)}, bf16[256,256]{1,0:T(8,128)(2,1)}, u32[]{:S(2)}) copy-start(bf16[256,256]{1,0:T(8,128)(2,1)} %param.12) | copy-start | bytes 393220
  167.5 7.2 %copy-start.5 = (f32[3,256]{1,0:T(4,128)S(1)}, f32[3,256]{1,0:T(4,128)}, u32[]{:S(2)}) copy-start(f32[3,256]{1,0:T(4,128)} %param.15) | copy-start | bytes 9220
  167.5 10.2 %copy-start.2 = (bf16[256,256]{1,0:T(8,128)(2,1)S(1)}, bf16[256,256]{1,0:T(8,128)(2,1)}, u32[]{:S(2)}) copy-start(bf16[256,256]{1,0:T(8,128)(2,1)} %param.13) | copy-start | bytes 393220
  167.5 62.4 %all-to-all-start.2 = ((bf16[4,320,2048]{2,1,0:T(8,128)(2,1)}), bf16[4,320,2048]{2,1,0:T(8,128)(2,1)}, u32[]{:S(2)}, u32[]{:S(2)}) async-start(bf16[4,320,2048]{2,1,0:T(8,128)(2,1)} %bitcast.49), calls=%async_computation.2 | async-start | bytes 10485760 | tf_op jit(solution)/shard_map/all_to_all | solution.py:40
  172.8 4.9 %collective-permute-start = (f32[2,256]{1,0:T(2,128)S(1)}, f32[2,256]{1,0:T(2,128)S(1)}, u32[]{:S(2)}, u32[]{:S(2)}) collective-permute-start(f32[2,256]{1,0:T(2,128)S(1)} %slice.36), channel_id=1, source_target_pairs={{0,4},{4,8},{8,12},{12,16},{16,20},{20,24},{24,28},{28,32},{32,36}... | collective-permute-start | bytes 6152 | tf_op jit(solution)/shard_map/ppermute | solution.py:30
  229.9 14.8 %all-to-all-start = ((bf16[4,64,2048]{2,1,0:T(8,128)(2,1)}), bf16[4,64,2048]{2,1,0:T(8,128)(2,1)S(1)}, u32[]{:S(2)}, u32[]{:S(2)}) async-start(bf16[4,64,2048]{2,1,0:T(8,128)(2,1)} %bitcast.3), calls=%async_computation | async-start | bytes 2097152 | tf_op jit(solution)/shard_map/all_to_all | solution.py:40
  237.0 22.3 %copy-start.6 = (f32[128,2]{0,1:T(2,128)S(1)}, f32[128,2]{0,1:T(2,128)}, u32[]{:S(2)}) copy-start(f32[128,2]{0,1:T(2,128)} %param.20) | copy-start | bytes 3076
  244.7 65.8 %all-to-all-start.3 = ((bf16[64,5,2048]{2,1,0:T(8,128)(2,1)}), bf16[64,5,2048]{2,1,0:T(8,128)(2,1)}, u32[]{:S(2)}, u32[]{:S(2)}) async-start(bf16[64,5,2048]{2,1,0:T(8,128)(2,1)} %reshape.91), calls=%async_computation.3 | async-start | bytes 4194304 | tf_op jit(solution)/shard_map/all_to_all | solution.py:114
